TPU v7x, 32 devices: a whole 2x2x4 slice. The times are simulated.
32 devices in a mesh: rep: 4 (over z), fs: 4 (over y, x), tp: 2 (over core).
Axes of the slice: x: 2, y: 2, z: 4, core: 2. Of those that a mesh axis runs over, the one named last changes fastest.
Arguments:
- inputs: bfloat16 [512, 2048], P(('rep', 'fs', 'tp')), may hold values from -6 to 6
- cotangent: bfloat16 [512, 2048], P(('rep', 'fs', 'tp')), may hold values from -6 to 6
- norm_gain: float32 [2048], replicated, may hold values from 0.1 to 1.9
- gate_weight: bfloat16 [2048, 2816], P(None, ('fs', 'tp')), may hold values from -0.125 to 0.125
- up_weight: bfloat16 [2048, 2816], P(None, ('fs', 'tp')), may hold values from -0.125 to 0.125
- down_weight: bfloat16 [2816, 2048], P(('fs', 'tp')), may hold values from -0.109375 to 0.109375
Outputs:
- input_grad: bfloat16 [512, 2048], P(('rep', 'fs', 'tp'))
- gain_grad: float32 [2048], replicated
- down_grad: float32 [2816, 2048], P(('fs', 'tp'), 'rep')
All inputs are finite; a program needn't handle non-finite values.
Results may differ from a plain program's by a relative error of at most 0.0066.
Values may be sent and summed in bfloat16 or wider, within the bound.
A program may use at most 64 MiB of HBM per device.

v0:
```python
import jax
import jax.numpy as jnp
from jax import lax
from jax.sharding import PartitionSpec as P

EPS = 1e-06


def across_tokens(left, right):
    return lax.dot_general(
        left, right, (((0,), (0,)), ((), ())), preferred_element_type=jnp.float32
    )


def across_columns(left, right):
    return lax.dot_general(
        left, right, (((1,), (1,)), ((), ())), preferred_element_type=jnp.float32
    )


def per_device(inputs, cotangent, norm_gain, gate_weight, up_weight, down_weight):
    whole_x, whole_dy = (
        lax.all_gather(inputs, ("fs", "tp"), axis=0, tiled=True),
        lax.all_gather(cotangent, ("fs", "tp"), axis=0, tiled=True),
    )
    xf = whole_x.astype(jnp.float32)
    inv = lax.rsqrt(jnp.mean(xf * xf, axis=-1, keepdims=True) + EPS)
    normed = xf * inv
    hidden_in = (normed * norm_gain).astype(jnp.bfloat16)
    gate = jnp.dot(hidden_in, gate_weight, preferred_element_type=jnp.float32)
    up = jnp.dot(hidden_in, up_weight, preferred_element_type=jnp.float32)
    sig = jax.nn.sigmoid(gate)
    act = gate * sig
    hidden = (act * up).astype(jnp.bfloat16)
    d_hidden = 0.5 * across_columns(whole_dy, down_weight)
    d_gate = (d_hidden * up * sig * (1.0 + gate * (1.0 - sig))).astype(jnp.bfloat16)
    d_up = (d_hidden * act).astype(jnp.bfloat16)
    own_rows = inputs.shape[0]
    d_in = lax.psum_scatter(
        across_columns(d_gate, gate_weight) + across_columns(d_up, up_weight),
        ("fs", "tp"),
        scatter_dimension=0,
        tiled=True,
    )
    offset = lax.axis_index(("fs", "tp")) * own_rows
    own_normed = lax.dynamic_slice_in_dim(normed, offset, own_rows, 0)
    own_inv = lax.dynamic_slice_in_dim(inv, offset, own_rows, 0)
    gain_grad = lax.psum(jnp.sum(d_in * own_normed, axis=0), ("rep", "fs", "tp"))
    scaled = d_in * norm_gain
    input_grad = (
        own_inv * (scaled - own_normed * jnp.mean(scaled * own_normed, axis=-1, keepdims=True))
    ).astype(jnp.bfloat16)
    input_grad, gain_grad = (input_grad, gain_grad)
    part_down = 0.5 * across_tokens(whole_dy, hidden)
    got_down = lax.all_to_all(
        part_down[None].astype(jnp.bfloat16), "rep", split_axis=1, concat_axis=0, tiled=True
    ).astype(jnp.float32)
    down_grad = jnp.sum(got_down, axis=0).T
    return (input_grad, gain_grad, down_grad)


def solution(mesh):
    return jax.shard_map(
        per_device,
        mesh=mesh,
        in_specs=(
            P(("rep", "fs", "tp"), None),
            P(("rep", "fs", "tp"), None),
            P(),
            P(None, ("fs", "tp")),
            P(None, ("fs", "tp")),
            P(("fs", "tp"), None),
        ),
        out_specs=(P(("rep", "fs", "tp"), None), P(), P(("fs", "tp"), "rep")),
        check_vma=False,
    )
```

profile of v0, /device:TPU:0, one launch (start us, length us, event | category | flops | bytes accessed | tf_op | source)
XLA Modules:
  0.0 166.7 jit_solution(2304956729085242355)
XLA Ops:
  7.2 11.8 %all_gather.6 = bf16[128,2048]{1,0:T(8,128)(2,1)S(1)} all-gather(bf16[16,2048]{1,0:T(8,128)(2,1)} %param.6), channel_id=1, replica_groups=mesh['rep'=4,'fs'=4,'tp'=2] {'fs','tp'}, dimensions={0}, use_global_device_ids=true | all-gather | bytes 589824 | tf_op jit(solution)/shard_map/all_gather | solution.py:23
  19.0 0.2 fusion.2
  19.2 1.4 fusion.3
  20.7 0.6 fusion.4
  21.3 0.3 copy-done.6
  21.6 9.5 %all_gather.7 = bf16[128,2048]{1,0:T(8,128)(2,1)S(1)} all-gather(bf16[16,2048]{1,0:T(8,128)(2,1)S(1)} %copy-done.6), channel_id=1, replica_groups=mesh['rep'=4,'fs'=4,'tp'=2] {'fs','tp'}, dimensions={0}, use_global_device_ids=true | all-gather | bytes 589824 | tf_op jit(solution)/shard_map/all_gather | solution.py:24
  31.1 0.8 copy-done.1
  31.9 0.5 convolution_multiply_fusion.1
  32.4 0.5 fusion.6
  33.0 1.5 convolution_add_fusion
  34.5 1.8 %fusion.1 = bf16[1,2048,352]{1,2,0:T(8,128)(2,1)S(1)} fusion(bf16[128,2048]{1,0:T(8,128)(2,1)} %copy-done.1, f32[128,352]{0,1:T(8,128)} %copy-done.5, f32[128,352]{0,1:T(8,128)} %copy-done.2), kind=kOutput, calls=%fused_computation.2 | convolution fusion | flops 186261504 | bytes 2326528 | tf_op jit(solution)/shard_map/dot_general | solution.py:10
  36.3 5.7 %copy.12 = bf16[1,2048,352]{2,0,1:T(2,128)(2,1)} copy(bf16[1,2048,352]{1,2,0:T(8,128)(2,1)S(1)} %fusion.1) | data formatting | bytes 2883584 | tf_op jit(solution)/shard_map/convert_element_type | solution.py:56
  42.0 0.5 broadcast.53
  42.5 34.4 %reduce = bf16[2048,352]{1,0:T(8,128)(2,1)S(1)} reduce(bf16[2048,1,352]{2,1,0:T(2,128)(2,1)} %bitcast.16, bf16[]{:T(256)} %broadcast.53), dimensions={1}, to_apply=%bitcast.7.reduce_sub_computation | reduce | bytes 2883586
  76.9 3.6 %reshape.41 = bf16[4,2,90112]{2,1,0:T(2,128)(2,1)} reshape(bf16[2048,352]{1,0:T(8,128)(2,1)S(1)} %reduce) | data formatting | bytes 2883584
  80.5 4.9 %all-to-all-start = ((bf16[4,2,90112]{2,1,0:T(2,128)(2,1)}), bf16[4,2,90112]{2,1,0:T(2,128)(2,1)S(1)}, u32[]{:S(2)}, u32[]{:S(2)}) async-start(bf16[4,2,90112]{2,1,0:T(2,128)(2,1)} %reshape.41), calls=%async_computation.1 | async-start | bytes 2883584 | tf_op jit(solution)/shard_map/all_to_all | solution.py:55
  85.4 1.1 convert_multiply_fusion
  86.5 1.1 multiply_reduce_fusion
  87.6 51.7 %psum.7 = f32[2048]{0:T(1024)} all-reduce(f32[2048]{0:T(1024)S(1)} %get-tuple-element.3), channel_id=1, replica_groups=mesh['rep'=4,'fs'=4,'tp'=2] {'rep','fs','tp'}, use_global_device_ids=true, to_apply=%region_4.0 | all-reduce | flops 2048 | bytes 16384 | tf_op jit(solution)/shard_map/psum | solution.py:48
  139.4 1.7 %multiply_convert_fusion.6 = bf16[16,2048]{1,0:T(8,128)(2,1)} fusion(f32[16,2048]{1,0:T(8,128)} %reduce-scatter.2.cloned.1.call-done, f32[128,2048]{1,0:T(8,128)} %convert_multiply_fusion, s32[]{:T(128)S(6)} %select_n.4, f32[16]{0:T(128)S(1)} %broadcast_multiply_fusion, f32[2048]{0:T(1024)S(1)} %copy-done.7, f32[16]{0:T(128)S(1)} %dynamic-slice.3), kind=kLoop, calls=%fused_computation.17 | loop fusion | flops 163840 | bytes 336004 | tf_op jit(solution)/shard_map/convert_element_type | solution.py:52
  141.1 4.0 %reshape.42 = bf16[2048,1,352]{2,1,0:T(2,128)(2,1)} reshape(bf16[4,2,90112]{2,1,0:T(2,128)(2,1)S(1)} %all-to-all-done) | data formatting | bytes 2883584
  145.0 7.0 %copy.13 = bf16[1,2048,352]{1,2,0:T(8,128)(2,1)S(1)} copy(bf16[1,2048,352]{2,0,1:T(2,128)(2,1)} %bitcast.17) | data formatting | bytes 2883584 | tf_op jit(solution)/shard_map/all_to_all | solution.py:55
  152.0 3.4 %reshape.40 = f32[4,512,352]{1,0,2:T(4,128)} reshape(bf16[1,2048,352]{1,2,0:T(8,128)(2,1)S(1)} %copy.13) | data formatting | bytes 4325376 | tf_op jit(solution)/shard_map/convert_element_type | solution.py:57
  155.5 4.4 %reduce_sum.39 = f32[512,352]{0,1:T(8,128)} reduce(f32[4,512,352]{1,0,2:T(4,128)} %reshape.40, f32[]{:T(128)} %constant.11.clone.1), dimensions={0}, to_apply=%region_5.0 | reduce | flops 540672 | bytes 3604484 | tf_op jit(solution)/shard_map/reduce_sum | solution.py:58
  (21 shorter events, 0.2 us)
Async XLA Ops:
  7.2 12.0 %copy-start = (bf16[2048,352]{0,1:T(8,128)(2,1)S(1)}, bf16[2048,352]{0,1:T(8,128)(2,1)}, u32[]{:S(2)}) copy-start(bf16[2048,352]{0,1:T(8,128)(2,1)} %param.9) | copy-start | bytes 4325380
  7.2 79.3 %reduce-scatter.2.cloned.1.call-start = ((), (), s32[]{:S(2)}) async-start(), calls=%async_computation.2 | async-start | bytes 1179648 | tf_op jit(solution)/shard_map/reduce_scatter | solution.py:39
  19.0 1.6 copy-start.4
  19.0 1.6 copy-start.7
  20.6 12.3 %copy-start.2 = (f32[128,352]{0,1:T(8,128)}, f32[128,352]{0,1:T(8,128)S(1)}, u32[]{:S(2)}) copy-start(f32[128,352]{0,1:T(8,128)S(1)} %fusion.3) | copy-start | bytes 540676
  20.6 0.9 copy-start.6
  20.7 11.2 %copy-start.3 = (bf16[352,2048]{1,0:T(8,128)(2,1)S(1)}, bf16[352,2048]{1,0:T(8,128)(2,1)}, u32[]{:S(2)}) copy-start(bf16[352,2048]{1,0:T(8,128)(2,1)} %param.11) | copy-start | bytes 4325380
  21.6 11.4 %copy-start.5 = (f32[128,352]{0,1:T(8,128)}, f32[128,352]{0,1:T(8,128)S(1)}, u32[]{:S(2)}) copy-start(f32[128,352]{0,1:T(8,128)S(1)} %fusion.4) | copy-start | bytes 540676
  31.1 0.8 copy-start.1
  80.5 60.6 %all-to-all-start = ((bf16[4,2,90112]{2,1,0:T(2,128)(2,1)}), bf16[4,2,90112]{2,1,0:T(2,128)(2,1)S(1)}, u32[]{:S(2)}, u32[]{:S(2)}) async-start(bf16[4,2,90112]{2,1,0:T(2,128)(2,1)} %reshape.41), calls=%async_computation.1 | async-start | bytes 2883584 | tf_op jit(solution)/shard_map/all_to_all | solution.py:55
Sparse Core Ops, SparseCore 0:
  34.6 36.2 reduce-scatter.1
where the time goes:
time: 167 us
  blocking collectives  73 us (44%)
  other arithmetic  42.9 us (26%)
  local copies, waits for them, and re-layouts  25.4 us (15%)
  between operations  14.2 us (9%)
  matrix products  6.35 us (4%)
  starting transfers between devices  4.91 us (3%)
    psum x1, blocking collectives, per_device(): lax.psum(jnp.sum(d_in * own_normed, axis=0), ('rep', 'fs', 'tp'))  51.7 us
    unnamed x1, other arithmetic  34.4 us
    all_gather x1, blocking collectives, per_device(): lax.all_gather(inputs, ('fs', 'tp'), axis=0, tiled=True)  11.8 us
    all_gather x1, blocking collectives, per_device(): lax.all_gather(cotangent, ('fs', 'tp'), axis=0, tiled=True)  9.52 us
    unnamed x19, local copies, waits for them, and re-layouts  9.19 us
    all_to_all x1, local copies, waits for them, and re-layouts, per_device(): lax.all_to_all(part_down[None].astype(jnp.bfloat16), 'rep', split_axis=1,...  7.01 us
    convert_element_type x1, local copies, waits for them, and re-layouts, per_device(): part_down[None].astype(jnp.bfloat16)  5.72 us
    all_to_all x1, starting transfers between devices, per_device(): lax.all_to_all(part_down[None].astype(jnp.bfloat16), 'rep', split_axis=1,...  4.87 us
  transfers between devices with their start and end apart: 2, of which 0 were waited for; matrix products, arithmetic and copies ran while one was open for 30% of the time, Pallas kernels for 0%

commit v1 on v0

--- a/solution.py
+++ b/solution.py
@@ -4,6 +4,12 @@
 from jax.sharding import PartitionSpec as P
 
 EPS = 1e-06
+
+
+def trade_parts(value, mesh_axis, split, join):
+    pieces = jnp.split(value, lax.axis_size(mesh_axis), axis=split)
+    arrived = lax.all_to_all(jnp.stack(pieces), mesh_axis, 0, 0)
+    return jnp.concatenate(arrived, axis=join)
 
 
 def across_tokens(left, right):
@@ -52,9 +58,7 @@
     ).astype(jnp.bfloat16)
     input_grad, gain_grad = (input_grad, gain_grad)
     part_down = 0.5 * across_tokens(whole_dy, hidden)
-    got_down = lax.all_to_all(
-        part_down[None].astype(jnp.bfloat16), "rep", split_axis=1, concat_axis=0, tiled=True
-    ).astype(jnp.float32)
+    got_down = trade_parts(part_down[None].astype(jnp.bfloat16), "rep", 1, 0).astype(jnp.float32)
     down_grad = jnp.sum(got_down, axis=0).T
     return (input_grad, gain_grad, down_grad)
 

time: 167 us -> 120 us (0.72)
  other arithmetic: 42.9 us -> 6.47 us
  waiting for transfers between devices: 0.02 us -> 28.4 us
  local copies, waits for them, and re-layouts: 25.4 us -> 0.95 us
  blocking collectives: 73 us -> 60.8 us
  matrix products: 6.35 us -> 4.33 us
    unnamed x1 -> x0, other arithmetic: 34.4 us -> none
    reduce_scatter x1, waiting for transfers between devices: 0.01 us -> 28.4 us  [per_device(): lax.psum_scatter(across_columns(d_gate, gate_weight) + across_columns(d_u...]
    psum x1, blocking collectives: 51.7 us -> 39.4 us  [per_device(): lax.psum(jnp.sum(d_in * own_normed, axis=0), ('rep', 'fs', 'tp'))]
    convert_element_type x2 -> x0, local copies, waits for them, and re-layouts: 9.15 us -> none  [the longest x1 5.72 us: per_device(): part_down[None].astype(jnp.bfloat16)]
    unnamed x19 -> x8, local copies, waits for them, and re-layouts: 9.19 us -> 0.75 us
    all_to_all x1 -> x0, local copies, waits for them, and re-layouts: 7.01 us -> none  [per_device(): lax.all_to_all(part_down[None].astype(jnp.bfloat16), 'rep', split_axis=1,...]
    reduce_sum x1, other arithmetic: 4.38 us -> 1.07 us  [per_device(): down_grad = jnp.sum(got_down, axis=0).T]
  transfers between devices with their start and end apart: 2 -> 2, of which waited for: 0 -> 1; matrix products, arithmetic and copies ran while one was open for 30% -> 5% of each run, Pallas kernels for 0% -> 0%
where the time goes in v1:
time: 120 us
  blocking collectives  60.8 us (51%)
  waiting for transfers between devices  28.4 us (24%)
  between operations  14.1 us (12%)
  other arithmetic  6.47 us (5%)
  starting transfers between devices  4.88 us (4%)
  matrix products  4.33 us (4%)
    psum x1, blocking collectives, per_device(): lax.psum(jnp.sum(d_in * own_normed, axis=0), ('rep', 'fs', 'tp'))  39.4 us
    reduce_scatter x1, waiting for transfers between devices, per_device(): lax.psum_scatter(across_columns(d_gate, gate_weight) + across_columns(d_u...  28.4 us
    all_gather x1, blocking collectives, per_device(): lax.all_gather(inputs, ('fs', 'tp'), axis=0, tiled=True)  11.8 us
    all_gather x1, blocking collectives, per_device(): lax.all_gather(cotangent, ('fs', 'tp'), axis=0, tiled=True)  9.67 us
    all_to_all x1, starting transfers between devices, trade_parts(): arrived = lax.all_to_all(jnp.stack(pieces), mesh_axis, 0, 0)  4.85 us
    dot_general x3, matrix products, across_columns(): lax.dot_general(left, right, (((1,), (1,)), ((), ())), preferred_element_...  2.56 us
  transfers between devices with their start and end apart: 2, of which 1 were waited for; matrix products, arithmetic and copies ran while one was open for 5% of the time, Pallas kernels for 0%

profile of v1, /device:TPU:0, one launch (start us, length us, event | category | flops | bytes accessed | tf_op | source)
XLA Modules:
  0.0 119.9 jit_solution(9823612420348382070)
XLA Ops:
  7.2 0.0 copy-start
  7.2 0.0 reduce-scatter.2.cloned.1.call-start
  7.2 11.8 %all_gather.6 = bf16[128,2048]{1,0:T(8,128)(2,1)S(1)} all-gather(bf16[16,2048]{1,0:T(8,128)(2,1)} %param.6), channel_id=1, replica_groups=mesh['rep'=4,'fs'=4,'tp'=2] {'fs','tp'}, dimensions={0}, use_global_device_ids=true | all-gather | bytes 589824 | tf_op jit(solution)/shard_map/all_gather | solution.py:29
  19.0 0.2 fusion.2
  19.2 9.7 %all_gather.7 = bf16[128,2048]{1,0:T(8,128)(2,1)S(1)} all-gather(bf16[16,2048]{1,0:T(8,128)(2,1)} %param.7), channel_id=1, replica_groups=mesh['rep'=4,'fs'=4,'tp'=2] {'fs','tp'}, dimensions={0}, use_global_device_ids=true | all-gather | bytes 589824 | tf_op jit(solution)/shard_map/all_gather | solution.py:30
  28.9 0.6 fusion.3
  29.5 0.0 copy-start.1
  29.5 0.6 fusion.4
  30.1 0.7 copy-done.1
  30.9 0.5 convolution_multiply_fusion.1
  31.4 0.5 fusion.6
  32.0 1.5 %convolution_add_fusion = f32[128,2048]{1,0:T(8,128)} fusion(f32[128,2048]{1,0:T(8,128)S(1)} %fusion.6, bf16[2048,352]{0,1:T(8,128)(2,1)S(1)} %copy-done.2, f32[128,352]{0,1:T(8,128)S(1)} %convolution_multiply_fusion.1, f32[128,352]{0,1:T(8,128)S(1)} %fusion.3), kind=kOutput, calls=%fused_computation.4 | convolution fusion | flops 185081856 | bytes 3899392 | tf_op jit(solution)/shard_map/dot_general | solution.py:22
  33.4 0.0 reduce-scatter.2.cloned.1.call-update
  33.5 0.5 fusion.1
  34.0 0.1 slice_bitcast_fusion.3
  34.1 1.3 %pad_maximum_fusion = bf16[4,1,512,352]{2,3,1,0:T(8,128)(2,1)} fusion(bf16[1,1,512,352]{2,3,1,0:T(8,128)(2,1)S(1)} %get-tuple-element.6, bf16[1,1,512,352]{2,3,1,0:T(8,128)(2,1)S(1)} %get-tuple-element.7, bf16[1,1,512,352]{2,3,1,0:T(8,128)(2,1)S(1)} %get-tuple-element.8, bf16[1,1,512,352]{2,3,1,0:T(8,128)(2,1)S(1)} %get-tuple-element.5), kind=kLoop, calls=%fused_computation.5 | loop fusion | flops 2162688 | bytes 2883584 | tf_op jit(solution)/shard_map/stack | solution.py:11
  35.4 4.8 %all-to-all-start = ((bf16[4,1,512,352]{2,3,1,0:T(8,128)(2,1)}), bf16[4,1,512,352]{2,3,1,0:T(8,128)(2,1)S(1)}, u32[]{:S(2)}, u32[]{:S(2)}) async-start(bf16[4,1,512,352]{2,3,1,0:T(8,128)(2,1)} %pad_maximum_fusion), calls=%async_computation.1 | async-start | bytes 2883584 | tf_op jit(solution)/shard_map/all_to_all | solution.py:11
  40.3 0.1 dynamic-slice.3
  40.4 1.1 convert_multiply_fusion
  41.5 28.4 %reduce-scatter.2.cloned.1.call-done = f32[16,2048]{1,0:T(8,128)} async-done(((f32[128,2048]{1,0:T(8,128)}), f32[16,2048]{1,0:T(8,128)}) %reduce-scatter.2.cloned.1.call-update) | async-done | bytes 131088 | tf_op jit(solution)/shard_map/reduce_scatter | solution.py:45
  69.8 1.1 multiply_reduce_fusion
  71.0 39.4 %psum.7 = f32[2048]{0:T(1024)} all-reduce(f32[2048]{0:T(1024)S(1)} %get-tuple-element.3), channel_id=1, replica_groups=mesh['rep'=4,'fs'=4,'tp'=2] {'rep','fs','tp'}, use_global_device_ids=true, to_apply=%region_4.0 | all-reduce | flops 2048 | bytes 16384 | tf_op jit(solution)/shard_map/psum | solution.py:54
  110.3 1.7 %multiply_convert_fusion.6 = bf16[16,2048]{1,0:T(8,128)(2,1)} fusion(f32[16,2048]{1,0:T(8,128)} %reduce-scatter.2.cloned.1.call-done, f32[128,2048]{1,0:T(8,128)} %convert_multiply_fusion, s32[]{:T(128)S(6)} %select_n.4, f32[16]{0:T(128)S(1)} %broadcast_multiply_fusion, f32[2048]{0:T(1024)S(1)} %copy-done.3, f32[16]{0:T(128)S(1)} %dynamic-slice.3), kind=kLoop, calls=%fused_computation.23 | loop fusion | flops 163840 | bytes 336004 | tf_op jit(solution)/shard_map/convert_element_type | solution.py:58
  112.0 1.1 convert_reduce_fusion
  (8 shorter events, 0.0 us)
Async XLA Ops:
  7.2 21.7 %copy-start = (bf16[2048,352]{0,1:T(8,128)(2,1)S(1)}, bf16[2048,352]{0,1:T(8,128)(2,1)}, u32[]{:S(2)}) copy-start(bf16[2048,352]{0,1:T(8,128)(2,1)} %param.9) | copy-start | bytes 4325380
  7.2 21.7 %copy-start.3 = (f32[2048]{0:T(1024)S(1)}, f32[2048]{0:T(1024)}, u32[]{:S(2)}) copy-start(f32[2048]{0:T(1024)} %param.8) | copy-start | bytes 24580
  7.2 62.6 %reduce-scatter.2.cloned.1.call-start = ((), (), s32[]{:S(2)}) async-start(), calls=%async_computation.2 | async-start | bytes 1179648 | tf_op jit(solution)/shard_map/reduce_scatter | solution.py:45
  19.2 10.3 %copy-start.2 = (bf16[2048,352]{0,1:T(8,128)(2,1)S(1)}, bf16[2048,352]{0,1:T(8,128)(2,1)}, u32[]{:S(2)}) copy-start(bf16[2048,352]{0,1:T(8,128)(2,1)} %param.10) | copy-start | bytes 4325380
  29.5 1.4 %copy-start.1 = (bf16[352,2048]{1,0:T(8,128)(2,1)S(1)}, bf16[352,2048]{1,0:T(8,128)(2,1)}, u32[]{:S(2)}) copy-start(bf16[352,2048]{1,0:T(8,128)(2,1)} %param.11) | copy-start | bytes 4325380
  35.4 76.5 %all-to-all-start = ((bf16[4,1,512,352]{2,3,1,0:T(8,128)(2,1)}), bf16[4,1,512,352]{2,3,1,0:T(8,128)(2,1)S(1)}, u32[]{:S(2)}, u32[]{:S(2)}) async-start(bf16[4,1,512,352]{2,3,1,0:T(8,128)(2,1)} %pad_maximum_fusion), calls=%async_computation.1 | async-start | bytes 2883584 | tf_op jit(solution)/shard_map/all_to_all | solution.py:11
Sparse Core Ops, SparseCore 0:
  33.6 36.2 reduce-scatter.1
